TPU v7x, 32 devices: a whole 2x2x4 slice. The times are simulated.
32 devices in a mesh: rep: 4 (over z), fs: 4 (over y, x), tp: 2 (over core).
Axes of the slice: x: 2, y: 2, z: 4, core: 2. Of those that a mesh axis runs over, the one named last changes fastest.
Arguments:
- hidden_pre: bfloat16 [8192, 4096], P(('rep', 'fs'), 'tp'), may hold values from -6 to 6
- out_grad: bfloat16 [8192, 2048], P(('rep', 'fs')), may hold values from -8 to 8
- down_weight: bfloat16 [2048, 4096], P('fs', 'tp'), may hold values from -0.09375 to 0.09375
Outputs:
- hidden_grad: bfloat16 [8192, 4096], P(('rep', 'fs'), 'tp')
- weight_grad: float32 [2048, 4096], P('fs', 'tp')
All inputs are finite; a program needn't handle non-finite values.
Results may differ from a plain program's by a relative error of at most 0.0049.
Values may be sent and summed in bfloat16 or wider, within the bound.
A program may use at most 64 MiB of HBM per device.

v0:
```python
import math
import jax
import jax.numpy as jnp
from jax import lax
from jax.sharding import PartitionSpec as P


def body(hidden_pre, out_grad, down_weight):
    rows = hidden_pre.shape[0]
    ff_local = hidden_pre.shape[1]
    back = jnp.dot(
        out_grad,
        lax.all_gather(down_weight, "fs", axis=0, tiled=True),
        preferred_element_type=jnp.float32,
    )
    positive = jnp.maximum(hidden_pre.astype(jnp.float32), 0.0)
    hidden_grad = (2.0 * positive * back).astype(jnp.bfloat16)
    act = (positive * positive).astype(jnp.bfloat16)
    partial_value = lax.dot_general(
        out_grad, act, (((0,), (0,)), ((), ())), preferred_element_type=jnp.float32
    )
    partial_value = partial_value.astype(jnp.bfloat16)
    received = lax.all_to_all(partial_value, "fs", split_axis=0, concat_axis=0, tiled=True)
    groups = lax.axis_size("fs")
    local_sum = jnp.sum(
        received.reshape(groups, received.shape[0] // groups, ff_local), axis=0, dtype=jnp.float32
    )
    total = lax.psum(local_sum, "rep")
    tokens_all = rows * lax.axis_size("rep") * groups
    weight_grad = total * (1.0 / math.sqrt(tokens_all))
    return (hidden_grad, weight_grad)


def solution(mesh):
    placed = (P(("rep", "fs"), "tp"), P(("rep", "fs"), None), P("fs", "tp"))
    return jax.shard_map(
        body,
        mesh=mesh,
        in_specs=placed,
        out_specs=(P(("rep", "fs"), "tp"), P("fs", "tp")),
        check_vma=False,
    )
```

profile of v0, /device:TPU:0, one launch (start us, length us, event | category | flops | bytes accessed | tf_op | source)
XLA Modules:
  0.0 297.2 jit_solution(1170586137731124309)
XLA Ops:
  8.0 0.0 copy-start
  8.0 0.0 all-reduce.2.cloned.1.call-start
  8.1 1.5 copy-done
  9.6 8.3 %convolution_convert_fusion = bf16[2048,2048]{0,1:T(8,128)(2,1)} fusion(bf16[512,2048]{1,0:T(8,128)(2,1)S(1)} %copy-done, bf16[512,2048]{1,0:T(8,128)(2,1)} %param.3), kind=kOutput, calls=%fused_computation.1 | convolution fusion | flops 4303355904 | bytes 12582912 | tf_op jit(solution)/shard_map/dot_general | solution.py:19
  17.9 98.5 %all_to_all.9 = bf16[4,512,2048]{2,1,0:T(8,128)(2,1)S(1)} all-to-all(bf16[4,512,2048]{2,1,0:T(8,128)(2,1)} %bitcast.6), channel_id=1, replica_groups=mesh['rep'=4,'fs'=4,'tp'=2] {'fs'}, dimensions={0} | all-to-all | bytes 16777216 | tf_op jit(solution)/shard_map/all_to_all | solution.py:23
  116.4 3.9 %convert_reduce_fusion = f32[512,2048]{1,0:T(8,128)} fusion(bf16[4,512,2048]{2,1,0:T(8,128)(2,1)S(1)} %all_to_all.9), kind=kLoop, calls=%fused_computation | loop fusion | flops 7340032 | bytes 12582912 | tf_op jit(solution)/shard_map/reduce_sum | solution.py:25
  120.3 0.0 all-reduce.2.cloned.1.call-update
  120.3 0.0 all-gather.2.cloned.1.call-start
  120.4 0.5 all-gather.2.cloned.1.call-update
  120.9 154.4 %all-reduce.2.cloned.1.call-done = f32[512,2048]{1,0:T(8,128)} async-done(((f32[512,2048]{1,0:T(8,128)}), f32[512,2048]{1,0:T(8,128)}) %all-reduce.2.cloned.1.call-update) | async-done | bytes 4194320 | tf_op jit(solution)/shard_map/psum | solution.py:28
  275.4 5.0 %broadcast_multiply_fusion = f32[512,2048]{1,0:T(8,128)} fusion(f32[512,2048]{1,0:T(8,128)} %all-reduce.2.cloned.1.call-done), kind=kLoop, calls=%fused_computation.5 | loop fusion | flops 1048576 | bytes 8388608 | tf_op jit(solution)/shard_map/mul | solution.py:30
  280.3 0.0 all-gather.2.cloned.1.call-done
  280.3 9.5 %multiply_convert_fusion.1 = bf16[512,2048]{1,0:T(8,128)(2,1)} fusion(bf16[512,2048]{1,0:T(8,128)(2,1)} %param.3, bf16[512,2048]{1,0:T(8,128)(2,1)S(1)} %copy-done, bf16[2048,2048]{1,0:T(8,128)(2,1)} %all-gather.2.cloned.1.call-done), kind=kOutput, calls=%fused_computation.3 | convolution fusion | flops 4300210176 | bytes 14680064 | tf_op jit(solution)/shard_map/dot_general | solution.py:11
Async XLA Ops:
  8.0 1.6 copy-start
  8.0 267.3 %all-reduce.2.cloned.1.call-start = ((), (), s32[]{:S(2)}) async-start(), calls=%async_computation.2 | async-start | bytes 8388608 | tf_op jit(solution)/shard_map/psum | solution.py:28
  120.3 160.0 %all-gather.2.cloned.1.call-start = ((), (), s32[]{:S(2)}) async-start(), calls=%async_computation.1 | async-start | bytes 10485760 | tf_op jit(solution)/shard_map/all_gather | solution.py:13
Sparse Core Ops, SparseCore 0:
  120.4 154.8 all-reduce.1
Sparse Core Ops, SparseCore 1:
  122.7 87.2 all-gather.1
where the time goes:
time: 297 us
  waiting for transfers between devices  155 us (52%)
  blocking collectives  98.5 us (33%)
  matrix products  17.8 us (6%)
  between operations  15.5 us (5%)
  other arithmetic  8.83 us (3%)
    psum x1, waiting for transfers between devices, body(): total = lax.psum(local_sum, 'rep')  154 us
    all_to_all x1, blocking collectives, body(): lax.all_to_all(partial_value, 'fs', split_axis=0, concat_axis=0, tiled=True)  98.5 us
    dot_general x1, matrix products, body(): jnp.dot(out_grad, lax.all_gather(down_weight, 'fs', axis=0, tiled=True),...  9.45 us
    dot_general x1, matrix products, body(): lax.dot_general(out_grad, act, (((0,), (0,)), ((), ())), preferred_elemen...  8.35 us
  transfers between devices with their start and end apart: 2, of which 1 were waited for; matrix products, arithmetic and copies ran while one was open for 2% of the time, Pallas kernels for 0%

commit v1 on v0

--- a/solution.py
+++ b/solution.py
@@ -25,7 +25,9 @@
     local_sum = jnp.sum(
         received.reshape(groups, received.shape[0] // groups, ff_local), axis=0, dtype=jnp.float32
     )
-    total = lax.psum(local_sum, "rep")
+    total = local_sum
+    for hop in (1, 2):
+        total = total + lax.ppermute(total, "rep", [(dev, dev ^ hop) for dev in range(4)])
     tokens_all = rows * lax.axis_size("rep") * groups
     weight_grad = total * (1.0 / math.sqrt(tokens_all))
     return (hidden_grad, weight_grad)

time: 297 us -> 447 us (1.51)
  waiting for transfers between devices: 155 us -> 387 us
  blocking collectives: 98.5 us -> 0 us
  starting transfers between devices: 0.08 us -> 11 us
  other arithmetic: 8.83 us -> 15.1 us
    ppermute x0 -> x2, waiting for transfers between devices: none -> 255 us  [body(): lax.ppermute(total, 'rep', [(dev, dev ^ hop) for dev in range(4)])]
    psum x1 -> x0, waiting for transfers between devices: 154 us -> none  [body(): total = lax.psum(local_sum, 'rep')]
    all_to_all x0 -> x1, waiting for transfers between devices: none -> 131 us  [body(): lax.all_to_all(partial_value, 'fs', split_axis=0, concat_axis=0, tiled=True)]
    all_to_all x1 -> x0, blocking collectives: 98.5 us -> none  [body(): lax.all_to_all(partial_value, 'fs', split_axis=0, concat_axis=0, tiled=True)]
    all_to_all x0 -> x1, starting transfers between devices: none -> 5.66 us  [body(): lax.all_to_all(partial_value, 'fs', split_axis=0, concat_axis=0, tiled=True)]
    ppermute x0 -> x2, starting transfers between devices: none -> 5.33 us  [body(): lax.ppermute(total, 'rep', [(dev, dev ^ hop) for dev in range(4)])]
  transfers between devices with their start and end apart: 2 -> 4, of which waited for: 1 -> 3; matrix products, arithmetic and copies ran while one was open for 2% -> 4% of each run, Pallas kernels for 0% -> 0%
where the time goes in v1:
time: 447 us; the launch traced here: 446 us
  waiting for transfers between devices  387 us (87%)
  matrix products  17.8 us (4%)
  other arithmetic  15.1 us (3%)
  between operations  14.1 us (3%)
  starting transfers between devices  11 us (2%)
    ppermute x2, waiting for transfers between devices, body(): lax.ppermute(total, 'rep', [(dev, dev ^ hop) for dev in range(4)])  255 us
    all_to_all x1, waiting for transfers between devices, body(): lax.all_to_all(partial_value, 'fs', split_axis=0, concat_axis=0, tiled=True)  131 us
    dot_general x1, matrix products, body(): jnp.dot(out_grad, lax.all_gather(down_weight, 'fs', axis=0, tiled=True),...  9.45 us
  transfers between devices with their start and end apart: 4, of which 3 were waited for; matrix products, arithmetic and copies ran while one was open for 4% of the time, Pallas kernels for 0%

profile of v1, /device:TPU:0, one launch (start us, length us, event | category | flops | bytes accessed | tf_op | source)
XLA Modules:
  0.0 446.3 jit_solution(14446443577105886237)
XLA Ops:
  7.2 0.0 copy-start
  7.2 1.6 copy-done
  8.8 8.4 %convolution_convert_fusion = bf16[2048,2048]{0,1:T(8,128)(2,1)} fusion(bf16[512,2048]{1,0:T(8,128)(2,1)S(1)} %copy-done, bf16[512,2048]{1,0:T(8,128)(2,1)} %param.3), kind=kOutput, calls=%fused_computation.1 | convolution fusion | flops 4303355904 | bytes 12582912 | tf_op jit(solution)/shard_map/dot_general | solution.py:19
  17.1 5.7 %all-to-all-start = ((bf16[4,512,2048]{2,1,0:T(8,128)(2,1)}), bf16[4,512,2048]{2,1,0:T(8,128)(2,1)}, u32[]{:S(2)}, u32[]{:S(2)}) async-start(bf16[4,512,2048]{2,1,0:T(8,128)(2,1)} %bitcast.6), calls=%async_computation | async-start | bytes 16777216 | tf_op jit(solution)/shard_map/all_to_all | solution.py:23
  22.8 0.0 all-gather.2.cloned.1.call-start
  22.8 0.7 all-gather.2.cloned.1.call-update
  23.5 130.7 %all-to-all-done = bf16[4,512,2048]{2,1,0:T(8,128)(2,1)} async-done(((bf16[4,512,2048]{2,1,0:T(8,128)(2,1)}), bf16[4,512,2048]{2,1,0:T(8,128)(2,1)}, u32[]{:S(2)}, u32[]{:S(2)}) %all-to-all-start) | async-done | bytes 8388640 | tf_op jit(solution)/shard_map/all_to_all | solution.py:23
  154.2 5.7 %convert_reduce_fusion = f32[512,2048]{1,0:T(8,128)S(1)} fusion(bf16[4,512,2048]{2,1,0:T(8,128)(2,1)} %all-to-all-done), kind=kLoop, calls=%fused_computation | loop fusion | flops 7340032 | bytes 12582912 | tf_op jit(solution)/shard_map/reduce_sum | solution.py:25
  159.9 2.5 collective-permute-start
  162.4 87.7 %collective-permute-done = f32[512,2048]{1,0:T(8,128)S(1)} collective-permute-done((f32[512,2048]{1,0:T(8,128)S(1)}, f32[512,2048]{1,0:T(8,128)S(1)}, u32[]{:S(2)}, u32[]{:S(2)}) %collective-permute-start) | collective-permute-done | bytes 4194336 | tf_op jit(solution)/shard_map/ppermute | solution.py:30
  250.1 2.8 add.6
  252.8 2.8 collective-permute-start.1
  255.7 0.0 all-gather.2.cloned.1.call-done
  255.7 9.5 %multiply_convert_fusion.1 = bf16[512,2048]{1,0:T(8,128)(2,1)} fusion(bf16[512,2048]{1,0:T(8,128)(2,1)} %param.3, bf16[512,2048]{1,0:T(8,128)(2,1)S(1)} %copy-done, bf16[2048,2048]{1,0:T(8,128)(2,1)} %all-gather.2.cloned.1.call-done), kind=kOutput, calls=%fused_computation.4 | convolution fusion | flops 4300210176 | bytes 14680064 | tf_op jit(solution)/shard_map/dot_general | solution.py:11
  265.1 167.6 %collective-permute-done.1 = f32[512,2048]{1,0:T(8,128)} collective-permute-done((f32[512,2048]{1,0:T(8,128)}, f32[512,2048]{1,0:T(8,128)}, u32[]{:S(2)}, u32[]{:S(2)}) %collective-permute-start.1) | collective-permute-done | bytes 4194336 | tf_op jit(solution)/shard_map/ppermute | solution.py:30
  432.8 6.7 %add_multiply_fusion = f32[512,2048]{1,0:T(8,128)} fusion(f32[512,2048]{1,0:T(8,128)} %add.6, f32[512,2048]{1,0:T(8,128)} %collective-permute-done.1), kind=kLoop, calls=%fused_computation.2 | loop fusion | flops 2097152 | bytes 12582912 | tf_op jit(solution)/shard_map/mul | solution.py:32
Async XLA Ops:
  7.2 1.6 copy-start
  17.1 137.1 %all-to-all-start = ((bf16[4,512,2048]{2,1,0:T(8,128)(2,1)}), bf16[4,512,2048]{2,1,0:T(8,128)(2,1)}, u32[]{:S(2)}, u32[]{:S(2)}) async-start(bf16[4,512,2048]{2,1,0:T(8,128)(2,1)} %bitcast.6), calls=%async_computation | async-start | bytes 16777216 | tf_op jit(solution)/shard_map/all_to_all | solution.py:23
  22.8 232.9 %all-gather.2.cloned.1.call-start = ((), (), s32[]{:S(2)}) async-start(), calls=%async_computation.1 | async-start | bytes 10485760 | tf_op jit(solution)/shard_map/all_gather | solution.py:13
  159.9 90.2 %collective-permute-start = (f32[512,2048]{1,0:T(8,128)S(1)}, f32[512,2048]{1,0:T(8,128)S(1)}, u32[]{:S(2)}, u32[]{:S(2)}) collective-permute-start(f32[512,2048]{1,0:T(8,128)S(1)} %convert_reduce_fusion), channel_id=1, source_target_pairs={{0,8},{8,0},{16,24},{24,16},{1,9},{9,1},{17,25},{25,17},{2,10},{10... | collective-permute-start | bytes 12582920 | tf_op jit(solution)/shard_map/ppermute | solution.py:30
  252.8 179.9 %collective-permute-start.1 = (f32[512,2048]{1,0:T(8,128)}, f32[512,2048]{1,0:T(8,128)}, u32[]{:S(2)}, u32[]{:S(2)}) collective-permute-start(f32[512,2048]{1,0:T(8,128)} %add.6), channel_id=1, source_target_pairs={{0,16},{8,24},{16,0},{24,8},{1,17},{9,25},{17,1},{25,9},{2,18},{10... | collective-permute-start | bytes 12582920 | tf_op jit(solution)/shard_map/ppermute | solution.py:30
Sparse Core Ops, SparseCore 0:
  25.5 158.7 all-gather.1
